TPU v7x, 32 devices: a whole 2x2x4 slice. The times are simulated.
32 devices in a mesh: sp: 8 (over z, x), tp: 4 (over y, core).
Axes of the slice: x: 2, y: 2, z: 4, core: 2. Of those that a mesh axis runs over, the one named last changes fastest.
Arguments:
- queries: bfloat16 [8192, 2048], P('sp', 'tp'), may hold values from -16 to 16
- key_rows: bfloat16 [8192, 512], P('sp', 'tp'), may hold values from -16 to 16
- value_rows: bfloat16 [8192, 512], P('sp', 'tp'), may hold values from -6 to 6
- doc_ids: int32 [8192], P('sp'), may hold values from 0 to 3, never falling along the last dimension, each value on 1 to 4096 neighbouring positions
- sink_logit: float32 [32], P('tp'), may hold values from 3 to 7
- residual: bfloat16 [8192, 2048], P(('sp', 'tp')), may hold values from -6 to 6
- out_weight: bfloat16 [2048, 2048], P('tp'), may hold values from -3.5 to 3.5
- norm_gain: float32 [2048], replicated, may hold values from 0.1 to 1.9
- gate_weight: bfloat16 [8, 2048, 512], P('sp'), may hold values from -0.125 to 0.125
- up_weight: bfloat16 [8, 2048, 512], P('sp'), may hold values from -0.125 to 0.125
- down_weight: bfloat16 [8, 512, 2048], P('sp'), may hold values from -0.25 to 0.25
- routes: int32 [8192, 2], P(('sp', 'tp')), may hold values from 0 to 7, as said below
- route_weights: float32 [8192, 2], P(('sp', 'tp')), may hold values from 0.2 to 0.8
Outputs:
- mixed: bfloat16 [8192, 2048], P(('sp', 'tp'))
Inputs may be any that keep to these rules, and one draw needn't show every extreme that they name: `doc_ids`: never falls along the positions. `routes`: each aligned block of 256 rows names every expert exactly 64 times; the experts of one row differ and lie in one group of 2 consecutive numbers.
All inputs are finite; a program needn't handle non-finite values.
Results may differ from a plain program's by a relative error of at most 0.012.
Values may be sent and summed in bfloat16 or wider, within the bound.
A program may use at most 128 MiB of HBM per device.

v0:
```python
import jax
import jax.numpy as jnp
from jax import lax
from jax.sharding import PartitionSpec as P

HD = 64
WINDOW = 128
neg_fill = -1e30
eps_norm = 1e-06


def extended(block, sides, width):
    for axis, dim in sides:
        count = lax.axis_size(axis)
        forward = [(i, i + 1) for i in range(count - 1)]
        backward = [(target, source) for source, target in forward]
        low = lax.ppermute(
            lax.slice_in_dim(block, block.shape[dim] - width, None, axis=dim), axis, forward
        )
        high = lax.ppermute(lax.slice_in_dim(block, 0, width, axis=dim), axis, backward)
        block = jnp.concatenate([low, block, high], axis=dim)
    return block


def attend(
    query_part,
    key_part,
    value_part,
    query_docs,
    key_docs,
    query_start,
    key_start,
    sink_logit,
    extent,
):
    query_count = query_part.shape[0]
    key_count = key_part.shape[0]
    groups = key_part.shape[1] // HD
    head_ratio = sink_logit.shape[0] // groups
    query_heads = query_part.reshape(query_count, groups, head_ratio, HD)
    key_heads = key_part.reshape(key_count, groups, HD)
    value_heads = value_part.reshape(key_count, groups, HD)
    scores = jnp.einsum(
        "qgrd,kgd->grqk", query_heads, key_heads, preferred_element_type=jnp.float32
    ) * HD ** (-0.5)
    query_pos = query_start + jnp.arange(query_count, dtype=jnp.int32)
    key_pos = key_start + jnp.arange(key_count, dtype=jnp.int32)
    inside = (key_pos >= 0) & (key_pos < extent)
    allowed = (
        (jnp.abs(query_pos[:, None] - key_pos[None, :]) <= WINDOW)
        & (query_docs[:, None] == key_docs[None, :])
        & inside[None, :]
    )
    masked = jnp.where(allowed[None, None], scores, neg_fill)
    sink_col = sink_logit.reshape(groups, head_ratio)[:, :, None, None]
    row_top = jnp.maximum(jnp.max(masked, axis=3, keepdims=True), sink_col)
    exponent = jnp.where(allowed[None, None], jnp.exp(masked - row_top), 0.0)
    denominator = jnp.sum(exponent, axis=3, keepdims=True) + jnp.exp(sink_col - row_top)
    attn_weight = (exponent / denominator).astype(jnp.bfloat16)
    attended = jnp.einsum(
        "grqk,kgd->qgrd", attn_weight, value_heads, preferred_element_type=jnp.float32
    )
    return attended.astype(jnp.bfloat16).reshape(query_count, -1)


def fetch_margins(key_rows, value_rows, doc_float):
    return (
        extended(key_rows, (("sp", 0),), WINDOW),
        extended(value_rows, (("sp", 0),), WINDOW),
        extended(doc_float, (("sp", 0),), WINDOW),
    )


def per_device(
    queries,
    key_rows,
    value_rows,
    doc_ids,
    sink_logit,
    residual,
    out_weight,
    norm_gain,
    gate_weight,
    up_weight,
    down_weight,
    routes,
    route_weights,
):
    local_rows = queries.shape[0]
    anchor = lax.axis_index("sp") * local_rows
    extent = local_rows * lax.axis_size("sp")
    doc_float = doc_ids.astype(jnp.bfloat16)
    block_rows = min(512, local_rows)
    padded_keys, padded_values, padded_docs = fetch_margins(key_rows, value_rows, doc_float)
    block_parts = []
    for row_start in range(0, local_rows, block_rows):
        key_end = row_start + block_rows + 2 * WINDOW
        block_parts.append(
            attend(
                queries[row_start : row_start + block_rows],
                padded_keys[row_start:key_end],
                padded_values[row_start:key_end],
                doc_float[row_start : row_start + block_rows],
                padded_docs[row_start:key_end],
                anchor + row_start,
                anchor + row_start - WINDOW,
                sink_logit,
                extent,
            )
        )
    attended = jnp.concatenate(block_parts, axis=0)
    regrouped = lax.all_to_all(attended, "tp", split_axis=0, concat_axis=1, tiled=True)
    shard_rows = out_weight.shape[0]
    initial = jnp.zeros((regrouped.shape[0], out_weight.shape[1]), jnp.float32)
    running = initial
    weight_piece = lax.all_gather(out_weight, "tp", axis=0, tiled=True)
    for shard_index in range(weight_piece.shape[0] // shard_rows):
        columns = lax.dynamic_slice_in_dim(regrouped, shard_index * shard_rows, shard_rows, 1)
        partial_value = jnp.dot(
            columns,
            weight_piece[shard_index * shard_rows : (shard_index + 1) * shard_rows],
            preferred_element_type=jnp.float32,
        )
        running = running + partial_value.astype(jnp.bfloat16).astype(jnp.float32)
    stream = (residual.astype(jnp.float32) + running).astype(jnp.bfloat16)
    stream_f = stream.astype(jnp.float32)
    scale = lax.rsqrt(jnp.mean(stream_f * stream_f, axis=1, keepdims=True) + eps_norm)
    normed = (stream_f * scale * norm_gain[None, :]).astype(jnp.bfloat16)
    home_rows = normed.shape[0]
    width = normed.shape[1]
    route_count = routes.shape[1]
    expert_count = lax.axis_size("sp") * gate_weight.shape[0]
    capacity = route_count * home_rows // expert_count
    flat_routes = routes.reshape(-1)
    one_hot = (flat_routes[:, None] == jnp.arange(expert_count, dtype=jnp.int32)[None, :]).astype(
        jnp.int32
    )
    earlier = jnp.cumsum(one_hot, axis=0) - one_hot
    slot_rank = jnp.sum(earlier * one_hot, axis=1)
    slot_index = flat_routes * capacity + slot_rank
    source_row = (
        jnp.zeros((expert_count * capacity,), jnp.int32)
        .at[slot_index]
        .set(jnp.arange(home_rows * route_count, dtype=jnp.int32) // route_count)
    )
    outgoing = normed[source_row].reshape(expert_count, capacity, width)
    incoming = lax.all_to_all(outgoing, "sp", split_axis=0, concat_axis=0, tiled=True)
    flat_rows = incoming.reshape(-1, width)
    gate_act = jnp.dot(flat_rows, gate_weight[0], preferred_element_type=jnp.float32)
    up_act = jnp.dot(flat_rows, up_weight[0], preferred_element_type=jnp.float32)
    hidden = (jax.nn.silu(gate_act) * up_act).astype(jnp.bfloat16)
    produced = jnp.dot(hidden, down_weight[0], preferred_element_type=jnp.float32).astype(
        jnp.bfloat16
    )
    returned = lax.all_to_all(
        produced.reshape(incoming.shape), "sp", split_axis=0, concat_axis=0, tiled=True
    )
    route_out = returned.reshape(-1, width)[slot_index].reshape(home_rows, route_count, width)
    weighted = jnp.sum(route_weights[:, :, None] * route_out.astype(jnp.float32), axis=1)
    return (stream_f + weighted).astype(jnp.bfloat16)


def solution(mesh):
    return jax.shard_map(
        per_device,
        mesh=mesh,
        in_specs=(
            P("sp", "tp"),
            P("sp", "tp"),
            P("sp", "tp"),
            P("sp"),
            P("tp"),
            P(("sp", "tp"), None),
            P("tp", None),
            P(),
            P("sp", None, None),
            P("sp", None, None),
            P("sp", None, None),
            P(("sp", "tp"), None),
            P(("sp", "tp"), None),
        ),
        out_specs=P(("sp", "tp"), None),
        check_vma=False,
    )
```

profile of v0, /device:TPU:0, one launch (start us, length us, event | category | flops | bytes accessed | tf_op | source)
XLA Modules:
  0.0 266.3 jit_solution(878454835703081858)
XLA Ops:
  8.0 4.9 %collective-permute-start.1 = (bf16[128]{0:T(256)(128)(2,1)S(1)}, bf16[128]{0:T(256)(128)(2,1)S(1)}, u32[]{:S(2)}, u32[]{:S(2)}) collective-permute-start(bf16[128]{0:T(256)(128)(2,1)S(1)} %get-tuple-element.17), channel_id=1, source_target_pairs={{0,4},{4,8},{8,12},{12,16},{16,20},{20,24},{24,28},{1,5},{5,9},{9,... | collective-permute-start | bytes 776 | tf_op jit(solution)/shard_map/ppermute | solution.py:17
  14.1 1.4 fusion.63
  15.5 4.5 %collective-permute-start.2 = (bf16[128,128]{1,0:T(8,128)(2,1)}, bf16[128,128]{1,0:T(8,128)(2,1)S(1)}, u32[]{:S(2)}, u32[]{:S(2)}) collective-permute-start(bf16[128,128]{1,0:T(8,128)(2,1)} %get-tuple-element.9), channel_id=1, source_target_pairs={{0,4},{4,8},{8,12},{12,16},{16,20},{20,24},{24,28},{1,5},{5,9},{9,... | collective-permute-start | bytes 98312 | tf_op jit(solution)/shard_map/ppermute | solution.py:17
  21.4 1.4 fusion.64
  22.8 5.0 %collective-permute-start = (bf16[128,128]{1,0:T(8,128)(2,1)}, bf16[128,128]{1,0:T(8,128)(2,1)S(1)}, u32[]{:S(2)}, u32[]{:S(2)}) collective-permute-start(bf16[128,128]{1,0:T(8,128)(2,1)} %get-tuple-element.13), channel_id=1, source_target_pairs={{0,4},{4,8},{8,12},{12,16},{16,20},{20,24},{24,28},{1,5},{5,9},{9,... | collective-permute-start | bytes 98312 | tf_op jit(solution)/shard_map/ppermute | solution.py:17
  41.6 2.4 fusion.30
  44.0 1.8 pad_maximum_fusion.3
  45.7 1.7 copy.36
  47.5 1.7 copy.40
  49.2 1.8 pad_maximum_fusion.4
  51.0 1.7 copy.35
  52.8 3.1 %fusion = (f32[2,4,512]{2,1,0:T(4,128)S(1)}, f32[2,768,512,4]{2,1,3,0:T(8,128)S(1)}) fusion(pred[512,768]{0,1:T(8,128)(4,1)S(1)} %get-tuple-element.30, bf16[768,2,64,1]{0,2,3,1:T(8,128)(2,1)} %bitcast.107, bf16[512,2,4,64]{0,3,2,1:T(8,128)(2,1)S(1)} %bitcast.104), kind=kOutput, calls=%fused_computation.9 | convolution fusion | flops 412086272 | bytes 13713408 | tf_op jit(solution)/shard_map/qgrd,kgd->grqk/dot_general | solution.py:43
  55.9 6.6 %fusion.1 = (f32[2,4,512]{2,1,0:T(4,128)S(1)}, f32[2,768,512,4]{2,1,3,0:T(8,128)}) fusion(pred[512,768]{0,1:T(8,128)(4,1)S(1)} %get-tuple-element.29, bf16[768,2,64,1]{0,2,3,1:T(8,128)(2,1)S(1)} %bitcast.106, bf16[512,2,4,64]{0,3,2,1:T(8,128)(2,1)S(1)} %bitcast.105), kind=kOutput, calls=%fused_computation.10 | convolution fusion | flops 412086272 | bytes 13713408 | tf_op jit(solution)/shard_map/qgrd,kgd->grqk/dot_general | solution.py:43
  62.5 3.1 %fusion.2 = f32[2,4,512]{2,1,0:T(4,128)S(1)} fusion(f32[2,768,512,4]{2,1,3,0:T(8,128)S(1)} %get-tuple-element.24, f32[2,4,512]{2,1,0:T(4,128)S(1)} %broadcast_maximum_fusion.1, pred[512,768]{0,1:T(8,128)(4,1)S(1)} %get-tuple-element.30), kind=kLoop, calls=%fused_computation.11 | loop fusion | flops 15724544 | bytes 13008896 | tf_op jit(solution)/shard_map/reduce_sum | solution.py:58
  65.7 4.7 %fusion.39 = bf16[2,64,4,512]{3,1,2,0:T(8,128)(2,1)} fusion(bf16[768,2,64,1]{0,2,3,1:T(8,128)(2,1)S(1)} %bitcast.110, f32[2,768,512,4]{2,1,3,0:T(8,128)S(1)} %get-tuple-element.24, f32[2,4,512]{2,1,0:T(4,128)S(1)} %get-tuple-element.21, f32[2,4,512]{2,1,0:T(4,128)S(1)} %broadcast_maximum_fusion.1, pred[512,768]{0,1:T(8,128)(4,1)S(1)} %get-tuple-element.30), kind=kOutput, calls=%fused_computation.55 | convolution fusion | flops 421789696 | bytes 13729792 | tf_op jit(solution)/shard_map/grqk,kgd->qgrd/dot_general | solution.py:60
  71.8 6.8 %fusion.3 = f32[2,4,512]{2,1,0:T(4,128)S(1)} fusion(f32[2,768,512,4]{2,1,3,0:T(8,128)} %get-tuple-element.26, f32[2,4,512]{2,1,0:T(4,128)S(1)} %get-tuple-element.22, pred[512,768]{0,1:T(8,128)(4,1)S(1)} %get-tuple-element.29), kind=kLoop, calls=%fused_computation.12 | loop fusion | flops 15724544 | bytes 13008896 | tf_op jit(solution)/shard_map/reduce_sum | solution.py:58
  80.1 4.6 %fusion.38 = bf16[2,64,4,512]{3,1,2,0:T(8,128)(2,1)} fusion(bf16[768,2,64,1]{0,2,3,1:T(8,128)(2,1)S(1)} %bitcast.111, f32[2,768,512,4]{2,1,3,0:T(8,128)S(1)} %copy-done.1, f32[2,4,512]{2,1,0:T(4,128)S(1)} %exponential_add_fusion, f32[2,4,512]{2,1,0:T(4,128)S(1)} %get-tuple-element.22, pred[512,768]{0,1:T(8,128)(4,1)S(1)} %get-tuple-element.29), kind=kOutput, calls=%fused_computation.54 | convolution fusion | flops 421789696 | bytes 13729792 | tf_op jit(solution)/shard_map/grqk,kgd->qgrd/dot_general | solution.py:60
  87.0 3.8 %all-to-all-start = ((bf16[4,256,512]{2,1,0:T(8,128)(2,1)}), bf16[4,256,512]{2,1,0:T(8,128)(2,1)S(1)}, u32[]{:S(2)}, u32[]{:S(2)}) async-start(bf16[4,256,512]{2,1,0:T(8,128)(2,1)} %bitcast.100), calls=%async_computation | async-start | bytes 2097152 | tf_op jit(solution)/shard_map/all_to_all | solution.py:112
  91.0 2.4 scatter_custom_fusion
  93.4 11.6 %all-to-all-done = bf16[4,256,512]{2,1,0:T(8,128)(2,1)S(1)} async-done(((bf16[4,256,512]{2,1,0:T(8,128)(2,1)}), bf16[4,256,512]{2,1,0:T(8,128)(2,1)S(1)}, u32[]{:S(2)}, u32[]{:S(2)}) %all-to-all-start) | async-done | bytes 1048608 | tf_op jit(solution)/shard_map/all_to_all | solution.py:112
  106.0 1.5 copy.45
  107.5 2.5 fusion.12
  110.0 2.9 %fusion.13 = f32[256,2048]{1,0:T(8,128)S(1)} fusion(bf16[2048,2048]{1,0:T(8,128)(2,1)} %all-gather.2.cloned.1.call-done, bf16[256,2048]{0,1:T(8,128)(2,1)S(1)} %bitcast.96), kind=kOutput, calls=%fused_computation.31 | convolution fusion | flops 537919488 | bytes 4456448 | tf_op jit(solution)/shard_map/dot_general | solution.py:119
  116.6 3.3 %gather_fusion = bf16[512,2048]{1,0:T(8,128)(2,1)} fusion(bf16[256,2048]{1,0:T(8,128)(2,1)S(1)} %fusion.17, s32[1024]{0:T(1024)S(1)} %pad_clamp_fusion.1), kind=kCustom, calls=%fused_computation | custom fusion | bytes 4196352 | tf_op jit(solution)/shard_map/gather | solution.py:146
  119.9 56.4 %all_to_all.29 = bf16[8,64,2048]{2,1,0:T(8,128)(2,1)S(1)} all-to-all(bf16[8,64,2048]{2,1,0:T(8,128)(2,1)} %bitcast.94), channel_id=1, replica_groups=mesh['sp'=8,'tp'=4] {'sp'}, dimensions={0} | all-to-all | bytes 4194304 | tf_op jit(solution)/shard_map/all_to_all | solution.py:147
  176.3 1.3 copy-done.6
  178.9 6.0 %convolution_convert_fusion = bf16[512,2048]{1,0:T(8,128)(2,1)} fusion(bf16[1,512,2048]{2,1,0:T(8,128)(2,1)S(1)} %copy-done, bf16[512,2048]{1,0:T(8,128)(2,1)} %bitcast.103, bf16[1,2048,512]{2,1,0:T(8,128)(2,1)} %param.22, f32[512,512]{1,0:T(8,128)S(1)} %fusion.26), kind=kOutput, calls=%fused_computation.19 | convolution fusion | flops 2150105088 | bytes 9437184 | tf_op jit(solution)/shard_map/dot_general | solution.py:152
  184.9 4.7 %all-to-all-start.2 = ((bf16[8,64,2048]{2,1,0:T(8,128)(2,1)}), bf16[8,64,2048]{2,1,0:T(8,128)(2,1)}, u32[]{:S(2)}, u32[]{:S(2)}) async-start(bf16[8,64,2048]{2,1,0:T(8,128)(2,1)} %bitcast.101), calls=%async_computation.2 | async-start | bytes 4194304 | tf_op jit(solution)/shard_map/all_to_all | solution.py:155
  189.8 46.9 %all-to-all-done.2 = bf16[8,64,2048]{2,1,0:T(8,128)(2,1)} async-done(((bf16[8,64,2048]{2,1,0:T(8,128)(2,1)}), bf16[8,64,2048]{2,1,0:T(8,128)(2,1)}, u32[]{:S(2)}, u32[]{:S(2)}) %all-to-all-start.2) | async-done | bytes 2097184 | tf_op jit(solution)/shard_map/all_to_all | solution.py:155
  236.7 7.1 %gather_fusion.1 = bf16[512,2048]{1,0:T(8,128)(2,1)} fusion(bf16[512,2048]{1,0:T(8,128)(2,1)} %bitcast.33, s32[1024]{0:T(1024)S(1)} %pad_clamp_fusion), kind=kCustom, calls=%fused_computation.1 | custom fusion | bytes 4196352 | tf_op jit(solution)/shard_map/gather | solution.py:158
  243.8 5.4 %reshape.312 = f32[256,2,2048]{2,1,0:T(2,128)} reshape(bf16[512,2048]{1,0:T(8,128)(2,1)} %gather_fusion.1) | data formatting | bytes 6291456 | tf_op jit(solution)/shard_map/convert_element_type | solution.py:159
  249.2 9.0 %multiply_reduce_fusion = f32[256,2048]{1,0:T(8,128)S(1)} fusion(f32[256,2,2048]{2,1,0:T(2,128)} %reshape.312, f32[256,2]{1,0:T(8,128)S(1)} %copy.46), kind=kLoop, calls=%fused_computation.15 | loop fusion | flops 1572864 | bytes 6293504 | tf_op jit(solution)/shard_map/reduce_sum | solution.py:159
  (107 shorter events, 30.5 us)
Async XLA Ops:
  6.5 172.4 %copy-start = (bf16[1,512,2048]{2,1,0:T(8,128)(2,1)S(1)}, bf16[1,512,2048]{2,1,0:T(8,128)(2,1)}, u32[]{:S(2)}) copy-start(bf16[1,512,2048]{2,1,0:T(8,128)(2,1)} %param.23) | copy-start | bytes 6291460
  6.5 21.2 %copy-start.18 = (s32[256,2]{0,1:T(2,128)S(1)}, s32[256,2]{0,1:T(2,128)}, u32[]{:S(2)}) copy-start(s32[256,2]{0,1:T(2,128)} %param.24) | copy-start | bytes 6148
  6.5 101.0 %all-gather.2.cloned.1.call-start = ((), (), s32[]{:S(2)}) async-start(), calls=%async_computation.3 | async-start | bytes 10485760 | tf_op jit(solution)/shard_map/all_gather | solution.py:116
  7.4 23.7 %copy-start.24 = (f32[8]{0:T(128)S(1)}, f32[8]{0:T(128)}, u32[]{:S(2)}) copy-start(f32[8]{0:T(128)} %param.17) | copy-start | bytes 100
  7.4 30.7 %copy-start.13 = (bf16[1024]{0:T(1024)(128)(2,1)}, bf16[1024]{0:T(1024)(128)(2,1)S(1)}, u32[]{:S(2)}) copy-start(bf16[1024]{0:T(1024)(128)(2,1)S(1)} %convert_element_type.80) | copy-start | bytes 6148
  8.0 31.1 %collective-permute-start.1 = (bf16[128]{0:T(256)(128)(2,1)S(1)}, bf16[128]{0:T(256)(128)(2,1)S(1)}, u32[]{:S(2)}, u32[]{:S(2)}) collective-permute-start(bf16[128]{0:T(256)(128)(2,1)S(1)} %get-tuple-element.17), channel_id=1, source_target_pairs={{0,4},{4,8},{8,12},{12,16},{16,20},{20,24},{24,28},{1,5},{5,9},{9,... | collective-permute-start | bytes 776 | tf_op jit(solution)/shard_map/ppermute | solution.py:17
  12.8 28.0 %collective-permute-start.4 = (bf16[128]{0:T(256)(128)(2,1)}, bf16[128]{0:T(256)(128)(2,1)}, u32[]{:S(2)}, u32[]{:S(2)}) collective-permute-start(bf16[128]{0:T(256)(128)(2,1)} %get-tuple-element.18), channel_id=1, source_target_pairs={{4,0},{8,4},{12,8},{16,12},{20,16},{24,20},{28,24},{5,1},{9,5},{13... | collective-permute-start | bytes 776 | tf_op jit(solution)/shard_map/ppermute | solution.py:20
  15.5 28.4 %collective-permute-start.2 = (bf16[128,128]{1,0:T(8,128)(2,1)}, bf16[128,128]{1,0:T(8,128)(2,1)S(1)}, u32[]{:S(2)}, u32[]{:S(2)}) collective-permute-start(bf16[128,128]{1,0:T(8,128)(2,1)} %get-tuple-element.9), channel_id=1, source_target_pairs={{0,4},{4,8},{8,12},{12,16},{16,20},{20,24},{24,28},{1,5},{5,9},{9,... | collective-permute-start | bytes 98312 | tf_op jit(solution)/shard_map/ppermute | solution.py:17
  20.1 23.9 %collective-permute-start.5 = (bf16[128,128]{1,0:T(8,128)(2,1)}, bf16[128,128]{1,0:T(8,128)(2,1)S(1)}, u32[]{:S(2)}, u32[]{:S(2)}) collective-permute-start(bf16[128,128]{1,0:T(8,128)(2,1)} %get-tuple-element.10), channel_id=1, source_target_pairs={{4,0},{8,4},{12,8},{16,12},{20,16},{24,20},{28,24},{5,1},{9,5},{13... | collective-permute-start | bytes 98312 | tf_op jit(solution)/shard_map/ppermute | solution.py:20
  22.8 26.5 %collective-permute-start = (bf16[128,128]{1,0:T(8,128)(2,1)}, bf16[128,128]{1,0:T(8,128)(2,1)S(1)}, u32[]{:S(2)}, u32[]{:S(2)}) collective-permute-start(bf16[128,128]{1,0:T(8,128)(2,1)} %get-tuple-element.13), channel_id=1, source_target_pairs={{0,4},{4,8},{8,12},{12,16},{16,20},{20,24},{24,28},{1,5},{5,9},{9,... | collective-permute-start | bytes 98312 | tf_op jit(solution)/shard_map/ppermute | solution.py:17
  38.1 14.7 %copy-start.7 = (bf16[512,512]{0,1:T(8,128)(2,1)S(1)}, bf16[512,512]{0,1:T(8,128)(2,1)}, u32[]{:S(2)}) copy-start(bf16[512,512]{0,1:T(8,128)(2,1)} %copy.37) | copy-start | bytes 1572868
  39.5 9.7 %collective-permute-start.3 = (bf16[128,128]{1,0:T(8,128)(2,1)}, bf16[128,128]{1,0:T(8,128)(2,1)S(1)}, u32[]{:S(2)}, u32[]{:S(2)}) collective-permute-start(bf16[128,128]{1,0:T(8,128)(2,1)} %get-tuple-element.14), channel_id=1, source_target_pairs={{4,0},{8,4},{12,8},{16,12},{20,16},{24,20},{28,24},{5,1},{9,5},{13... | collective-permute-start | bytes 98312 | tf_op jit(solution)/shard_map/ppermute | solution.py:20
  52.8 3.1 %copy-start.15 = (f32[2,4]{1,0:T(2,128)S(1)}, f32[2,4]{1,0:T(2,128)}, u32[]{:S(2)}) copy-start(f32[2,4]{1,0:T(2,128)} %max.32) | copy-start | bytes 100
  52.8 3.2 %copy-start.8 = (bf16[512,512]{0,1:T(8,128)(2,1)S(1)}, bf16[512,512]{0,1:T(8,128)(2,1)}, u32[]{:S(2)}) copy-start(bf16[512,512]{0,1:T(8,128)(2,1)} %copy.41) | copy-start | bytes 1572868
  52.8 3.2 %copy-start.11 = (bf16[768,128]{0,1:T(8,128)(2,1)S(1)}, bf16[768,128]{0,1:T(8,128)(2,1)}, u32[]{:S(2)}) copy-start(bf16[768,128]{0,1:T(8,128)(2,1)} %copy.40) | copy-start | bytes 589828
  62.5 3.2 %copy-start.12 = (bf16[768,128]{0,1:T(8,128)(2,1)S(1)}, bf16[768,128]{0,1:T(8,128)(2,1)}, u32[]{:S(2)}) copy-start(bf16[768,128]{0,1:T(8,128)(2,1)} %copy.35) | copy-start | bytes 589828
  65.7 5.9 %copy-start.10 = (bf16[768,128]{1,0:T(8,128)(2,1)S(1)}, bf16[768,128]{1,0:T(8,128)(2,1)}, u32[]{:S(2)}) copy-start(bf16[768,128]{1,0:T(8,128)(2,1)} %get-tuple-element.12) | copy-start | bytes 589828
  71.8 8.2 %copy-start.1 = (f32[2,768,512,4]{2,1,3,0:T(8,128)S(1)}, f32[2,768,512,4]{2,1,3,0:T(8,128)}, u32[]{:S(2)}) copy-start(f32[2,768,512,4]{2,1,3,0:T(8,128)} %get-tuple-element.26) | copy-start | bytes 37748740
  87.0 3.9 %slice-start = ((s32[8,5]{0,1:T(8,128)}), s32[8,4]{0,1:T(4,128)S(1)}, s32[]{:S(2)}) async-start(s32[8,5]{0,1:T(8,128)} %copy-done.14), calls=%async_computation.4 | async-start | bytes 4096 | tf_op jit(solution)/shard_map/slice.1
  87.0 3.9 %copy-start.19 = (s32[512]{0:T(512)S(1)}, s32[512]{0:T(512)}, u32[]{:S(2)}) copy-start(s32[512]{0:T(512)} %eq.65) | copy-start | bytes 6148
  87.0 4.0 %copy-start.17 = (s32[512,1]{0,1:T(1,128)S(1)}, s32[512,1]{0,1:T(1,128)}, u32[]{:S(2)}) copy-start(s32[512,1]{0,1:T(1,128)} %mul.81) | copy-start | bytes 6148
  87.0 18.1 %all-to-all-start = ((bf16[4,256,512]{2,1,0:T(8,128)(2,1)}), bf16[4,256,512]{2,1,0:T(8,128)(2,1)S(1)}, u32[]{:S(2)}, u32[]{:S(2)}) async-start(bf16[4,256,512]{2,1,0:T(8,128)(2,1)} %bitcast.100), calls=%async_computation | async-start | bytes 2097152 | tf_op jit(solution)/shard_map/all_to_all | solution.py:112
  105.1 1.0 copy-start.5
  107.5 5.3 %copy-start.4 = (bf16[2048,2048]{1,0:T(8,128)(2,1)S(1)}, bf16[2048,2048]{1,0:T(8,128)(2,1)}, u32[]{:S(2)}) copy-start(bf16[2048,2048]{1,0:T(8,128)(2,1)} %all-gather.2.cloned.1.call-done) | copy-start | bytes 25165828
  112.9 1.2 copy-start.9
  114.1 2.2 copy-start.16
  115.3 1.0 copy-start.2
  119.9 57.8 %copy-start.23 = (bf16[1,2048,512]{2,1,0:T(8,128)(2,1)S(1)}, bf16[1,2048,512]{2,1,0:T(8,128)(2,1)}, u32[]{:S(2)}) copy-start(bf16[1,2048,512]{2,1,0:T(8,128)(2,1)} %param.21) | copy-start | bytes 6291460
  176.3 1.3 copy-start.6
  184.9 4.7 %copy-start.21 = (f32[256,2]{0,1:T(2,128)S(1)}, f32[256,2]{0,1:T(2,128)}, u32[]{:S(2)}) copy-start(f32[256,2]{0,1:T(2,128)} %param.25) | copy-start | bytes 6148
  184.9 51.8 %all-to-all-start.2 = ((bf16[8,64,2048]{2,1,0:T(8,128)(2,1)}), bf16[8,64,2048]{2,1,0:T(8,128)(2,1)}, u32[]{:S(2)}, u32[]{:S(2)}) async-start(bf16[8,64,2048]{2,1,0:T(8,128)(2,1)} %bitcast.101), calls=%async_computation.2 | async-start | bytes 4194304 | tf_op jit(solution)/shard_map/all_to_all | solution.py:155
  249.2 9.0 %copy-start.3 = (bf16[256,2048]{1,0:T(8,128)(2,1)S(1)}, bf16[256,2048]{1,0:T(8,128)(2,1)}, u32[]{:S(2)}) copy-start(bf16[256,2048]{1,0:T(8,128)(2,1)} %copy-done.2) | copy-start | bytes 3145732
  (3 other events, 2.2 us)
Sparse Core Ops, SparseCore 0:
  8.9 60.9 all-gather.1
where the time goes:
time: 267 us; the launch traced here: 266 us
  waiting for transfers between devices  59.3 us (22%)
  blocking collectives  56.4 us (21%)
  local copies, waits for them, and re-layouts  43.4 us (16%)
  matrix products  33.4 us (13%)
  other arithmetic  33.2 us (12%)
  starting transfers between devices  26.8 us (10%)
  between operations  13.8 us (5%)
    all_to_all x1, blocking collectives, per_device(): lax.all_to_all(outgoing, 'sp', split_axis=0, concat_axis=0, tiled=True)  56.4 us
    all_to_all x1, waiting for transfers between devices, per_device(): lax.all_to_all(produced.reshape(incoming.shape), 'sp', split_axis=0, conc...  46.9 us
    ppermute x3, starting transfers between devices, extended(): lax.ppermute(lax.slice_in_dim(block, block.shape[dim] - width, None, axis...  14.4 us
    all_to_all x1, waiting for transfers between devices, per_device(): lax.all_to_all(attended, 'tp', split_axis=0, concat_axis=1, tiled=True)  11.6 us
    reduce_sum x2, other arithmetic, attend(): jnp.sum(exponent, axis=3, keepdims=True) + jnp.exp(sink_col - row_top)  9.89 us
    dot_general x2, matrix products, attend(): jnp.einsum('qgrd,kgd->grqk', query_heads, key_heads, preferred_element_ty...  9.67 us
    dot_general x2, matrix products, attend(): jnp.einsum('grqk,kgd->qgrd', attn_weight, value_heads, preferred_element_...  9.31 us
    reduce_sum x1, other arithmetic, per_device(): jnp.sum(route_weights[:, :, None] * route_out.astype(jnp.float32), axis=1)  8.96 us
  transfers between devices with their start and end apart: 9, of which 2 were waited for; matrix products, arithmetic and copies ran while one was open for 24% of the time, Pallas kernels for 0%

commit v1 on v0

--- a/solution.py
+++ b/solution.py
@@ -109,7 +109,10 @@
             )
         )
     attended = jnp.concatenate(block_parts, axis=0)
-    regrouped = lax.all_to_all(attended, "tp", split_axis=0, concat_axis=1, tiled=True)
+    regrouped = jnp.concatenate(
+        lax.all_to_all(jnp.stack(jnp.split(attended, lax.axis_size("tp"), axis=0)), "tp", 0, 0),
+        axis=1,
+    )
     shard_rows = out_weight.shape[0]
     initial = jnp.zeros((regrouped.shape[0], out_weight.shape[1]), jnp.float32)
     running = initial

time: 267 us -> 254 us (0.951)
  matrix products: 33.4 us -> 27.5 us
  local copies, waits for them, and re-layouts: 43.4 us -> 39.7 us
  other arithmetic: 33.2 us -> 29.6 us
    dot_general x2, matrix products: 9.67 us -> 5.18 us  [attend(): jnp.einsum('qgrd,kgd->grqk', query_heads, key_heads, preferred_element_ty...]
    reduce_sum x2, other arithmetic: 9.89 us -> 6.21 us  [attend(): jnp.sum(exponent, axis=3, keepdims=True) + jnp.exp(sink_col - row_top)]
    unnamed x52 -> x48, local copies, waits for them, and re-layouts: 6 us -> 3.81 us
  transfers between devices with their start and end apart: 9 -> 9, of which waited for: 2 -> 2; matrix products, arithmetic and copies ran while one was open for 24% -> 21% of each run, Pallas kernels for 0% -> 0%
where the time goes in v1:
time: 254 us; the launch traced here: 253 us
  waiting for transfers between devices  59.3 us (23%)
  blocking collectives  56.4 us (22%)
  local copies, waits for them, and re-layouts  39.7 us (16%)
  other arithmetic  29.6 us (12%)
  matrix products  27.5 us (11%)
  starting transfers between devices  26.6 us (10%)
  between operations  13.8 us (5%)
    all_to_all x1, blocking collectives, per_device(): lax.all_to_all(outgoing, 'sp', split_axis=0, concat_axis=0, tiled=True)  56.4 us
    all_to_all x1, waiting for transfers between devices, per_device(): lax.all_to_all(produced.reshape(incoming.shape), 'sp', split_axis=0, conc...  46.9 us
    ppermute x3, starting transfers between devices, extended(): lax.ppermute(lax.slice_in_dim(block, block.shape[dim] - width, None, axis...  14.4 us
    all_to_all x1, waiting for transfers between devices, per_device(): lax.all_to_all(jnp.stack(jnp.split(attended, lax.axis_size('tp'), axis=0)...  11.6 us
    reduce_sum x1, other arithmetic, per_device(): jnp.sum(route_weights[:, :, None] * route_out.astype(jnp.float32), axis=1)  8.96 us
    dot_general x2, matrix products, attend(): jnp.einsum('grqk,kgd->qgrd', attn_weight, value_heads, preferred_element_...  7.89 us
    dot_general x4, matrix products, per_device(): jnp.dot(columns, weight_piece[shard_index * shard_rows:(shard_index + 1)...  7.24 us
    gather x1, local copies, waits for them, and re-layouts, per_device(): returned.reshape(-1, width)[slot_index]  7.12 us
  transfers between devices with their start and end apart: 9, of which 2 were waited for; matrix products, arithmetic and copies ran while one was open for 21% of the time, Pallas kernels for 0%

profile of v1, /device:TPU:0, one launch (start us, length us, event | category | flops | bytes accessed | tf_op | source)
XLA Modules:
  0.0 253.0 jit_solution(16243603594748408)
XLA Ops:
  8.0 4.9 %collective-permute-start.1 = (bf16[128]{0:T(256)(128)(2,1)S(1)}, bf16[128]{0:T(256)(128)(2,1)S(1)}, u32[]{:S(2)}, u32[]{:S(2)}) collective-permute-start(bf16[128]{0:T(256)(128)(2,1)S(1)} %get-tuple-element.21), channel_id=1, source_target_pairs={{0,4},{4,8},{8,12},{12,16},{16,20},{20,24},{24,28},{1,5},{5,9},{9,... | collective-permute-start | bytes 776 | tf_op jit(solution)/shard_map/ppermute | solution.py:17
  14.1 1.4 fusion.67
  15.5 4.5 %collective-permute-start.2 = (bf16[128,128]{1,0:T(8,128)(2,1)}, bf16[128,128]{1,0:T(8,128)(2,1)S(1)}, u32[]{:S(2)}, u32[]{:S(2)}) collective-permute-start(bf16[128,128]{1,0:T(8,128)(2,1)} %get-tuple-element.13), channel_id=1, source_target_pairs={{0,4},{4,8},{8,12},{12,16},{16,20},{20,24},{24,28},{1,5},{5,9},{9,... | collective-permute-start | bytes 98312 | tf_op jit(solution)/shard_map/ppermute | solution.py:17
  21.4 1.4 fusion.68
  22.8 5.0 %collective-permute-start = (bf16[128,128]{1,0:T(8,128)(2,1)}, bf16[128,128]{1,0:T(8,128)(2,1)S(1)}, u32[]{:S(2)}, u32[]{:S(2)}) collective-permute-start(bf16[128,128]{1,0:T(8,128)(2,1)} %get-tuple-element.17), channel_id=1, source_target_pairs={{0,4},{4,8},{8,12},{12,16},{16,20},{20,24},{24,28},{1,5},{5,9},{9,... | collective-permute-start | bytes 98312 | tf_op jit(solution)/shard_map/ppermute | solution.py:17
  42.4 2.4 fusion.30
  44.8 1.8 pad_maximum_fusion.3
  46.5 1.8 copy.24
  48.3 1.8 copy.28
  50.1 1.8 pad_maximum_fusion.4
  51.9 1.7 copy.23
  53.6 1.7 copy.27
  55.3 3.1 %fusion = (f32[2,4,512]{2,1,0:T(4,128)S(1)}, f32[2,768,512,4]{2,1,3,0:T(8,128)S(1)}) fusion(pred[512,768]{0,1:T(8,128)(4,1)S(1)} %get-tuple-element.34, bf16[768,2,64,1]{0,2,3,1:T(8,128)(2,1)} %bitcast.115, bf16[512,2,4,64]{0,3,2,1:T(8,128)(2,1)S(1)} %bitcast.108), kind=kOutput, calls=%fused_computation.9 | convolution fusion | flops 412086272 | bytes 13713408 | tf_op jit(solution)/shard_map/qgrd,kgd->grqk/dot_general | solution.py:43
  58.5 2.1 fusion.1
  60.6 3.1 %fusion.2 = f32[2,4,512]{2,1,0:T(4,128)S(1)} fusion(f32[2,768,512,4]{2,1,3,0:T(8,128)S(1)} %get-tuple-element.28, f32[2,4,512]{2,1,0:T(4,128)S(1)} %broadcast_maximum_fusion.1, pred[512,768]{0,1:T(8,128)(4,1)S(1)} %get-tuple-element.34), kind=kLoop, calls=%fused_computation.11 | loop fusion | flops 15724544 | bytes 13008896 | tf_op jit(solution)/shard_map/reduce_sum | solution.py:58
  63.8 3.1 %fusion.3 = f32[2,4,512]{2,1,0:T(4,128)S(1)} fusion(f32[2,768,512,4]{2,1,3,0:T(8,128)S(1)} %get-tuple-element.30, f32[2,4,512]{2,1,0:T(4,128)S(1)} %get-tuple-element.26, pred[512,768]{0,1:T(8,128)(4,1)S(1)} %get-tuple-element.33), kind=kLoop, calls=%fused_computation.12 | loop fusion | flops 15724544 | bytes 13008896 | tf_op jit(solution)/shard_map/reduce_sum | solution.py:58
  67.0 3.9 %fusion.40 = bf16[512,2,4,64]{0,3,2,1:T(8,128)(2,1)S(1)} fusion(bf16[768,2,64,1]{0,2,3,1:T(8,128)(2,1)S(1)} %bitcast.117, f32[2,768,512,4]{2,1,3,0:T(8,128)S(1)} %get-tuple-element.28, f32[2,4,512]{2,1,0:T(4,128)S(1)} %get-tuple-element.25, f32[2,4,512]{2,1,0:T(4,128)S(1)} %broadcast_maximum_fusion.1, pred[512,768]{0,1:T(8,128)(4,1)S(1)} %get-tuple-element.34), kind=kOutput, calls=%fused_computation.56 | convolution fusion | flops 421789696 | bytes 13729792 | tf_op jit(solution)/shard_map/grqk,kgd->qgrd/dot_general | solution.py:60
  71.0 3.9 %fusion.41 = bf16[512,2,4,64]{0,3,2,1:T(8,128)(2,1)S(1)} fusion(bf16[768,2,64,1]{0,2,3,1:T(8,128)(2,1)S(1)} %bitcast.116, f32[2,768,512,4]{2,1,3,0:T(8,128)S(1)} %get-tuple-element.30, f32[2,4,512]{2,1,0:T(4,128)S(1)} %exponential_add_fusion, f32[2,4,512]{2,1,0:T(4,128)S(1)} %get-tuple-element.26, pred[512,768]{0,1:T(8,128)(4,1)S(1)} %get-tuple-element.33), kind=kOutput, calls=%fused_computation.57 | convolution fusion | flops 421789696 | bytes 13729792 | tf_op jit(solution)/shard_map/grqk,kgd->qgrd/dot_general | solution.py:60
  76.2 3.7 %all-to-all-start = ((bf16[4,256,512]{1,2,0:T(8,128)(2,1)}), bf16[4,256,512]{1,2,0:T(8,128)(2,1)S(1)}, u32[]{:S(2)}, u32[]{:S(2)}) async-start(bf16[4,256,512]{1,2,0:T(8,128)(2,1)} %pad_maximum_fusion), calls=%async_computation | async-start | bytes 2097152 | tf_op jit(solution)/shard_map/all_to_all | solution.py:113
  80.0 2.4 scatter_custom_fusion
  82.5 11.6 %all-to-all-done = bf16[4,256,512]{1,2,0:T(8,128)(2,1)S(1)} async-done(((bf16[4,256,512]{1,2,0:T(8,128)(2,1)}), bf16[4,256,512]{1,2,0:T(8,128)(2,1)S(1)}, u32[]{:S(2)}, u32[]{:S(2)}) %all-to-all-start) | async-done | bytes 1048608 | tf_op jit(solution)/shard_map/all_to_all | solution.py:113
  94.1 2.5 fusion.12
  96.6 2.9 %fusion.13 = f32[256,2048]{1,0:T(8,128)S(1)} fusion(bf16[2048,2048]{1,0:T(8,128)(2,1)} %all-gather.2.cloned.1.call-done, bf16[256,2048]{0,1:T(8,128)(2,1)S(1)} %bitcast.102), kind=kOutput, calls=%fused_computation.31 | convolution fusion | flops 537919488 | bytes 4456448 | tf_op jit(solution)/shard_map/dot_general | solution.py:122
  103.2 3.3 %gather_fusion = bf16[512,2048]{1,0:T(8,128)(2,1)} fusion(bf16[256,2048]{1,0:T(8,128)(2,1)S(1)} %fusion.17, s32[1024]{0:T(1024)S(1)} %pad_clamp_fusion.1), kind=kCustom, calls=%fused_computation | custom fusion | bytes 4196352 | tf_op jit(solution)/shard_map/gather | solution.py:149
  106.5 56.4 %all_to_all.15 = bf16[8,64,2048]{2,1,0:T(8,128)(2,1)S(1)} all-to-all(bf16[8,64,2048]{2,1,0:T(8,128)(2,1)} %bitcast.100), channel_id=1, replica_groups=mesh['sp'=8,'tp'=4] {'sp'}, dimensions={0} | all-to-all | bytes 4194304 | tf_op jit(solution)/shard_map/all_to_all | solution.py:150
  162.9 1.3 copy-done.4
  165.5 6.0 %convolution_convert_fusion = bf16[512,2048]{1,0:T(8,128)(2,1)} fusion(bf16[1,512,2048]{2,1,0:T(8,128)(2,1)S(1)} %copy-done, bf16[512,2048]{1,0:T(8,128)(2,1)} %bitcast.107, bf16[1,2048,512]{2,1,0:T(8,128)(2,1)} %param.22, f32[512,512]{1,0:T(8,128)S(1)} %fusion.26), kind=kOutput, calls=%fused_computation.19 | convolution fusion | flops 2150105088 | bytes 9437184 | tf_op jit(solution)/shard_map/dot_general | solution.py:155
  171.5 4.7 %all-to-all-start.2 = ((bf16[8,64,2048]{2,1,0:T(8,128)(2,1)}), bf16[8,64,2048]{2,1,0:T(8,128)(2,1)}, u32[]{:S(2)}, u32[]{:S(2)}) async-start(bf16[8,64,2048]{2,1,0:T(8,128)(2,1)} %bitcast.105), calls=%async_computation.2 | async-start | bytes 4194304 | tf_op jit(solution)/shard_map/all_to_all | solution.py:158
  176.4 46.9 %all-to-all-done.2 = bf16[8,64,2048]{2,1,0:T(8,128)(2,1)} async-done(((bf16[8,64,2048]{2,1,0:T(8,128)(2,1)}), bf16[8,64,2048]{2,1,0:T(8,128)(2,1)}, u32[]{:S(2)}, u32[]{:S(2)}) %all-to-all-start.2) | async-done | bytes 2097184 | tf_op jit(solution)/shard_map/all_to_all | solution.py:158
  223.3 7.1 %gather_fusion.1 = bf16[512,2048]{1,0:T(8,128)(2,1)} fusion(bf16[512,2048]{1,0:T(8,128)(2,1)} %bitcast.35, s32[1024]{0:T(1024)S(1)} %pad_clamp_fusion), kind=kCustom, calls=%fused_computation.1 | custom fusion | bytes 4196352 | tf_op jit(solution)/shard_map/gather | solution.py:161
  230.4 5.5 %reshape.319 = f32[256,2,2048]{2,1,0:T(2,128)} reshape(bf16[512,2048]{1,0:T(8,128)(2,1)} %gather_fusion.1) | data formatting | bytes 6291456 | tf_op jit(solution)/shard_map/convert_element_type | solution.py:162
  235.9 9.0 %multiply_reduce_fusion = f32[256,2048]{1,0:T(8,128)S(1)} fusion(f32[256,2,2048]{2,1,0:T(2,128)} %reshape.319, f32[256,2]{1,0:T(8,128)S(1)} %copy.31), kind=kLoop, calls=%fused_computation.15 | loop fusion | flops 1572864 | bytes 6293504 | tf_op jit(solution)/shard_map/reduce_sum | solution.py:162
  (101 shorter events, 26.5 us)
Async XLA Ops:
  6.5 159.0 %copy-start = (bf16[1,512,2048]{2,1,0:T(8,128)(2,1)S(1)}, bf16[1,512,2048]{2,1,0:T(8,128)(2,1)}, u32[]{:S(2)}) copy-start(bf16[1,512,2048]{2,1,0:T(8,128)(2,1)} %param.23) | copy-start | bytes 6291460
  6.5 0.8 copy-start.18
  6.5 21.2 %copy-start.15 = (s32[256,2]{0,1:T(2,128)S(1)}, s32[256,2]{0,1:T(2,128)}, u32[]{:S(2)}) copy-start(s32[256,2]{0,1:T(2,128)} %param.24) | copy-start | bytes 6148
  6.5 87.6 %all-gather.2.cloned.1.call-start = ((), (), s32[]{:S(2)}) async-start(), calls=%async_computation.3 | async-start | bytes 10485760 | tf_op jit(solution)/shard_map/all_gather | solution.py:119
  7.4 23.7 %copy-start.22 = (f32[8]{0:T(128)S(1)}, f32[8]{0:T(128)}, u32[]{:S(2)}) copy-start(f32[8]{0:T(128)} %param.17) | copy-start | bytes 100
  7.4 29.9 %copy-start.11 = (bf16[1024]{0:T(1024)(128)(2,1)}, bf16[1024]{0:T(1024)(128)(2,1)S(1)}, u32[]{:S(2)}) copy-start(bf16[1024]{0:T(1024)(128)(2,1)S(1)} %convert_element_type.80) | copy-start | bytes 6148
  8.0 31.8 %collective-permute-start.1 = (bf16[128]{0:T(256)(128)(2,1)S(1)}, bf16[128]{0:T(256)(128)(2,1)S(1)}, u32[]{:S(2)}, u32[]{:S(2)}) collective-permute-start(bf16[128]{0:T(256)(128)(2,1)S(1)} %get-tuple-element.21), channel_id=1, source_target_pairs={{0,4},{4,8},{8,12},{12,16},{16,20},{20,24},{24,28},{1,5},{5,9},{9,... | collective-permute-start | bytes 776 | tf_op jit(solution)/shard_map/ppermute | solution.py:17
  12.8 28.8 %collective-permute-start.4 = (bf16[128]{0:T(256)(128)(2,1)}, bf16[128]{0:T(256)(128)(2,1)}, u32[]{:S(2)}, u32[]{:S(2)}) collective-permute-start(bf16[128]{0:T(256)(128)(2,1)} %get-tuple-element.22), channel_id=1, source_target_pairs={{4,0},{8,4},{12,8},{16,12},{20,16},{24,20},{28,24},{5,1},{9,5},{13... | collective-permute-start | bytes 776 | tf_op jit(solution)/shard_map/ppermute | solution.py:20
  15.5 29.2 %collective-permute-start.2 = (bf16[128,128]{1,0:T(8,128)(2,1)}, bf16[128,128]{1,0:T(8,128)(2,1)S(1)}, u32[]{:S(2)}, u32[]{:S(2)}) collective-permute-start(bf16[128,128]{1,0:T(8,128)(2,1)} %get-tuple-element.13), channel_id=1, source_target_pairs={{0,4},{4,8},{8,12},{12,16},{16,20},{20,24},{24,28},{1,5},{5,9},{9,... | collective-permute-start | bytes 98312 | tf_op jit(solution)/shard_map/ppermute | solution.py:17
  20.1 24.7 %collective-permute-start.5 = (bf16[128,128]{1,0:T(8,128)(2,1)}, bf16[128,128]{1,0:T(8,128)(2,1)S(1)}, u32[]{:S(2)}, u32[]{:S(2)}) collective-permute-start(bf16[128,128]{1,0:T(8,128)(2,1)} %get-tuple-element.14), channel_id=1, source_target_pairs={{4,0},{8,4},{12,8},{16,12},{20,16},{24,20},{28,24},{5,1},{9,5},{13... | collective-permute-start | bytes 98312 | tf_op jit(solution)/shard_map/ppermute | solution.py:20
  22.8 27.3 %collective-permute-start = (bf16[128,128]{1,0:T(8,128)(2,1)}, bf16[128,128]{1,0:T(8,128)(2,1)S(1)}, u32[]{:S(2)}, u32[]{:S(2)}) collective-permute-start(bf16[128,128]{1,0:T(8,128)(2,1)} %get-tuple-element.17), channel_id=1, source_target_pairs={{0,4},{4,8},{8,12},{12,16},{16,20},{20,24},{24,28},{1,5},{5,9},{9,... | collective-permute-start | bytes 98312 | tf_op jit(solution)/shard_map/ppermute | solution.py:17
  38.3 17.1 %copy-start.5 = (bf16[512,512]{0,1:T(8,128)(2,1)S(1)}, bf16[512,512]{0,1:T(8,128)(2,1)}, u32[]{:S(2)}) copy-start(bf16[512,512]{0,1:T(8,128)(2,1)} %copy.25) | copy-start | bytes 1572868
  39.7 0.6 copy-start.20
  40.3 9.8 %collective-permute-start.3 = (bf16[128,128]{1,0:T(8,128)(2,1)}, bf16[128,128]{1,0:T(8,128)(2,1)S(1)}, u32[]{:S(2)}, u32[]{:S(2)}) collective-permute-start(bf16[128,128]{1,0:T(8,128)(2,1)} %get-tuple-element.18), channel_id=1, source_target_pairs={{4,0},{8,4},{12,8},{16,12},{20,16},{24,20},{28,24},{5,1},{9,5},{13... | collective-permute-start | bytes 98312 | tf_op jit(solution)/shard_map/ppermute | solution.py:20
  55.3 3.1 %copy-start.12 = (f32[2,4]{1,0:T(2,128)S(1)}, f32[2,4]{1,0:T(2,128)}, u32[]{:S(2)}) copy-start(f32[2,4]{1,0:T(2,128)} %max.32) | copy-start | bytes 100
  55.3 3.2 %copy-start.6 = (bf16[512,512]{0,1:T(8,128)(2,1)S(1)}, bf16[512,512]{0,1:T(8,128)(2,1)}, u32[]{:S(2)}) copy-start(bf16[512,512]{0,1:T(8,128)(2,1)} %copy.29) | copy-start | bytes 1572868
  55.3 3.2 %copy-start.8 = (bf16[768,128]{0,1:T(8,128)(2,1)S(1)}, bf16[768,128]{0,1:T(8,128)(2,1)}, u32[]{:S(2)}) copy-start(bf16[768,128]{0,1:T(8,128)(2,1)} %copy.28) | copy-start | bytes 589828
  63.8 3.2 %copy-start.10 = (bf16[768,128]{0,1:T(8,128)(2,1)S(1)}, bf16[768,128]{0,1:T(8,128)(2,1)}, u32[]{:S(2)}) copy-start(bf16[768,128]{0,1:T(8,128)(2,1)} %copy.23) | copy-start | bytes 589828
  67.0 4.0 %copy-start.9 = (bf16[768,128]{0,1:T(8,128)(2,1)S(1)}, bf16[768,128]{0,1:T(8,128)(2,1)}, u32[]{:S(2)}) copy-start(bf16[768,128]{0,1:T(8,128)(2,1)} %copy.27) | copy-start | bytes 589828
  75.1 4.9 %copy-start.16 = (s32[512]{0:T(512)S(1)}, s32[512]{0:T(512)}, u32[]{:S(2)}) copy-start(s32[512]{0:T(512)} %eq.65) | copy-start | bytes 6148
  75.1 4.9 %copy-start.17 = (s32[8,4]{0,1:T(4,128)S(1)}, s32[8,4]{0,1:T(4,128)}, u32[]{:S(2)}) copy-start(s32[8,4]{0,1:T(4,128)} %slice.97) | copy-start | bytes 388
  75.1 4.9 %copy-start.14 = (s32[512,1]{0,1:T(1,128)S(1)}, s32[512,1]{0,1:T(1,128)}, u32[]{:S(2)}) copy-start(s32[512,1]{0,1:T(1,128)} %mul.81) | copy-start | bytes 6148
  76.2 17.9 %all-to-all-start = ((bf16[4,256,512]{1,2,0:T(8,128)(2,1)}), bf16[4,256,512]{1,2,0:T(8,128)(2,1)S(1)}, u32[]{:S(2)}, u32[]{:S(2)}) async-start(bf16[4,256,512]{1,2,0:T(8,128)(2,1)} %pad_maximum_fusion), calls=%async_computation | async-start | bytes 2097152 | tf_op jit(solution)/shard_map/all_to_all | solution.py:113
  94.1 5.3 %copy-start.3 = (bf16[2048,2048]{1,0:T(8,128)(2,1)S(1)}, bf16[2048,2048]{1,0:T(8,128)(2,1)}, u32[]{:S(2)}) copy-start(bf16[2048,2048]{1,0:T(8,128)(2,1)} %all-gather.2.cloned.1.call-done) | copy-start | bytes 25165828
  99.5 1.2 copy-start.7
  100.7 2.2 copy-start.13
  101.9 1.0 copy-start.1
  106.5 57.8 %copy-start.21 = (bf16[1,2048,512]{2,1,0:T(8,128)(2,1)S(1)}, bf16[1,2048,512]{2,1,0:T(8,128)(2,1)}, u32[]{:S(2)}) copy-start(bf16[1,2048,512]{2,1,0:T(8,128)(2,1)} %param.21) | copy-start | bytes 6291460
  162.9 1.3 copy-start.4
  171.5 4.7 %copy-start.19 = (f32[256,2]{0,1:T(2,128)S(1)}, f32[256,2]{0,1:T(2,128)}, u32[]{:S(2)}) copy-start(f32[256,2]{0,1:T(2,128)} %param.25) | copy-start | bytes 6148
  171.5 51.8 %all-to-all-start.2 = ((bf16[8,64,2048]{2,1,0:T(8,128)(2,1)}), bf16[8,64,2048]{2,1,0:T(8,128)(2,1)}, u32[]{:S(2)}, u32[]{:S(2)}) async-start(bf16[8,64,2048]{2,1,0:T(8,128)(2,1)} %bitcast.105), calls=%async_computation.2 | async-start | bytes 4194304 | tf_op jit(solution)/shard_map/all_to_all | solution.py:158
  235.9 9.0 %copy-start.2 = (bf16[256,2048]{1,0:T(8,128)(2,1)S(1)}, bf16[256,2048]{1,0:T(8,128)(2,1)}, u32[]{:S(2)}) copy-start(bf16[256,2048]{1,0:T(8,128)(2,1)} %copy-done.1) | copy-start | bytes 3145732
Sparse Core Ops, SparseCore 0:
  8.9 60.9 all-gather.1
